TPU v7x, 256 devices: a 4x2x16 block of a 4x16x16 slice. The times are simulated.
256 devices in a mesh: grp: 2 (over y), ep: 32 (over z, core), tp: 4 (over x).
Axes of the slice: x: 4, y: 2, z: 16, core: 2. Of those that a mesh axis runs over, the one named last changes fastest.
The devices are a block of a 4x16x16 slice.
Arguments:
- outer_gate: bfloat16 [16384, 2048], P(('grp', 'ep'), 'tp'), parts along dimension 0, may hold values from -6 to 6
- inner_gate: bfloat16 [16384, 2048], P(('grp', 'ep'), 'tp'), parts along dimension 0, may hold values from -6 to 6
- inner_value: bfloat16 [16384, 2048], P(('grp', 'ep'), 'tp'), parts along dimension 0, may hold values from -6 to 6
- conv_taps: bfloat16 [3, 2048], replicated, may hold values from -3 to 3
- mixer_out: bfloat16 [2048, 2048], P('tp'), may hold values from -0.125 to 0.125
- mixer_gain: float32 [2048], replicated, may hold values from 0.1 to 1.9
- moe_tokens: bfloat16 [16384, 2048], P(('grp', 'ep', 'tp')), parts along dimension 0, may hold values from -6 to 6
- expert_gain: float32 [2048], replicated, may hold values from 0.1 to 1.9
- route_ids: int32 [16384, 4], P(('grp', 'ep', 'tp')), parts along dimension 0, may hold values from 0 to 127, all different within a row; in each aligned block of 64 rows (0 to 63, 64 to 127, ...) at most 3 rows name the same one
- route_weights: float32 [16384, 4], P(('grp', 'ep', 'tp')), parts along dimension 0, may hold values from 0.2 to 1
- expert_gate: bfloat16 [128, 2048, 512], P(('ep', 'tp')), may hold values from -0.125 to 0.125
- expert_up: bfloat16 [128, 2048, 512], P(('ep', 'tp')), may hold values from -0.125 to 0.125
- expert_down: bfloat16 [128, 512, 2048], P(('ep', 'tp')), may hold values from -0.25 to 0.25
- shared_gate: bfloat16 [2048, 512], P(None, 'tp'), may hold values from -0.125 to 0.125
- shared_up: bfloat16 [2048, 512], P(None, 'tp'), may hold values from -0.125 to 0.125
- shared_down: bfloat16 [512, 2048], P('tp'), may hold values from -0.25 to 0.25
Outputs:
- mixed_rows: bfloat16 [16384, 2048], P(('grp', 'ep', 'tp')), parts along dimension 0
- expert_rows: bfloat16 [16384, 2048], P(('grp', 'ep', 'tp')), parts along dimension 0
There are 2 independent parts, one for each index of `grp`. A program takes and returns all parts, laid end to end along the dimension named above; an argument that names none is the same for every part. Nothing has to cross between parts.
Inputs may be any that keep to these rules, and one draw needn't show every extreme that they name: `route_ids`: each row names 4 different experts; among the 64 rows of one device (aligned blocks) no expert is named more than 3 times, a bound that some block reaches.
All inputs are finite; a program needn't handle non-finite values.
Results may differ from a plain program's by a relative error of at most 0.012.
Values may be sent and summed in bfloat16 or wider, within the bound.
A program may use at most 64 MiB of HBM per device.

v0:
```python
import jax
import jax.numpy as jnp
from jax import lax
from jax.sharding import PartitionSpec as P

EPSILON = 1e-06


def passed_along(array, axis, by):
    size = lax.axis_size(axis)
    pairs = [(i, i + by) for i in range(size) if 0 <= i + by < size]
    return lax.ppermute(array, axis, pairs)


def laid_out(pieces, dim):
    shape = list(pieces.shape[1:])
    shape[dim] *= pieces.shape[0]
    return jnp.moveaxis(pieces, 0, dim).reshape(shape)


def work_in_pieces(array, axis, dim, apply, out_dim):
    size, span = (lax.axis_size(axis), array.shape[dim])
    count = 2 if span % 2 == 0 else 1
    outs, length = ([], span // count)
    for k in range(count):
        share = lax.slice_in_dim(array, k * length, (k + 1) * length, axis=dim)
        starts = jnp.arange(size) * span + k * length
        outs.append(jax.vmap(apply)(lax.all_gather(share, axis), starts))
    return laid_out(jnp.concatenate(outs, axis=out_dim + 1), out_dim)


def in_blocks(array, dim, size):
    shape = array.shape
    pieces = array.reshape(*shape[:dim], size, shape[dim] // size, *shape[dim + 1 :])
    return jnp.moveaxis(pieces, dim, 0)


def summed_on_arrival(array, axis, dim):
    pieces = in_blocks(array, dim, lax.axis_size(axis))
    arrived = lax.all_to_all(pieces, axis, split_axis=0, concat_axis=0, tiled=True)
    return arrived.astype(jnp.float32).sum(axis=0)


def rms_scale(values, gains):
    return values * lax.rsqrt(jnp.mean(values * values, axis=-1, keepdims=True) + EPSILON) * gains


def on_device(
    outer_gate,
    inner_gate,
    inner_value,
    conv_taps,
    mixer_out,
    mixer_gain,
    moe_tokens,
    expert_gain,
    route_ids,
    route_weights,
    expert_gate,
    expert_up,
    expert_down,
    shared_gate,
    shared_up,
    shared_down,
):
    columns = inner_gate.shape[1]
    kernel = lax.dynamic_slice_in_dim(conv_taps, lax.axis_index("tp") * columns, columns, 1).astype(
        jnp.float32
    )
    before_gate, before_value = passed_along((inner_gate[-2:], inner_value[-2:]), "ep", 1)
    gate_rows = jnp.concatenate([before_gate, inner_gate], axis=0).astype(jnp.float32)
    value_rows = jnp.concatenate([before_value, inner_value], axis=0).astype(jnp.float32)
    product = gate_rows * value_rows
    filtered = kernel[0] * product[:-2] + kernel[1] * product[1:-1] + kernel[2] * product[2:]
    scaled = (outer_gate.astype(jnp.float32) * filtered).astype(jnp.bfloat16)
    normed = rms_scale(moe_tokens.astype(jnp.float32), expert_gain).astype(jnp.bfloat16)
    feature_width = normed.shape[1]

    def shared_piece(piece, start):
        gate_value = jnp.dot(piece, shared_gate, preferred_element_type=jnp.float32)
        up_value = jnp.dot(piece, shared_up, preferred_element_type=jnp.float32)
        return (jax.nn.silu(gate_value) * up_value).astype(jnp.bfloat16)

    shared_act = work_in_pieces(normed, "tp", 0, shared_piece, 0)
    mixer_part = jnp.dot(scaled, mixer_out, preferred_element_type=jnp.float32)
    shared_part = jnp.dot(shared_act, shared_down, preferred_element_type=jnp.float32)
    both_sums = summed_on_arrival(
        jnp.concatenate([mixer_part, shared_part], axis=1).astype(jnp.bfloat16), "tp", 0
    )
    mixed_rows = rms_scale(both_sums[:, :feature_width], mixer_gain).astype(jnp.bfloat16)
    shared_out = both_sums[:, feature_width:]
    row_count, top_count = route_ids.shape
    ep_count = lax.axis_size("ep")
    tp_count = lax.axis_size("tp")
    expert_count = ep_count * tp_count
    capacity = (3 * row_count * top_count + 2 * expert_count - 1) // (2 * expert_count)
    flat_ids = route_ids.reshape(-1)
    onehot = (flat_ids[:, None] == jnp.arange(expert_count, dtype=jnp.int32)[None, :]).astype(
        jnp.int32
    )
    slot_rank = jnp.sum(
        (jnp.cumsum(onehot, axis=0, dtype=jnp.int32) - onehot) * onehot, axis=1, dtype=jnp.int32
    )
    target = flat_ids * capacity + slot_rank
    token_of = jnp.arange(flat_ids.shape[0], dtype=jnp.int32) // top_count
    slot_token = jnp.zeros((expert_count * capacity,), jnp.int32).at[target].set(token_of)
    outgoing = normed[slot_token].reshape(expert_count, capacity, feature_width)
    arrived = lax.all_to_all(outgoing, ("ep", "tp"), split_axis=0, concat_axis=0, tiled=True)
    flat_in = arrived.reshape(expert_count * capacity, feature_width)
    gate_value = jnp.dot(flat_in, expert_gate[0], preferred_element_type=jnp.float32)
    up_value = jnp.dot(flat_in, expert_up[0], preferred_element_type=jnp.float32)
    active = (jax.nn.silu(gate_value) * up_value).astype(jnp.bfloat16)
    result = jnp.dot(active, expert_down[0], preferred_element_type=jnp.float32).astype(
        jnp.bfloat16
    )
    returned = lax.all_to_all(
        result.reshape(expert_count, capacity, feature_width),
        ("ep", "tp"),
        split_axis=0,
        concat_axis=0,
        tiled=True,
    )
    picked = returned.reshape(expert_count * capacity, feature_width)[target].astype(jnp.float32)
    weights = route_weights.reshape(-1)
    routed = jnp.sum(
        (weights[:, None] * picked).reshape(row_count, top_count, feature_width), axis=1
    )
    expert_rows = (shared_out + routed).astype(jnp.bfloat16)
    return (mixed_rows, expert_rows)


def solution(mesh):
    return jax.shard_map(
        on_device,
        mesh=mesh,
        in_specs=(
            P(("grp", "ep"), "tp"),
            P(("grp", "ep"), "tp"),
            P(("grp", "ep"), "tp"),
            P(),
            P("tp", None),
            P(),
            P(("grp", "ep", "tp"), None),
            P(),
            P(("grp", "ep", "tp"), None),
            P(("grp", "ep", "tp"), None),
            P(("ep", "tp"), None, None),
            P(("ep", "tp"), None, None),
            P(("ep", "tp"), None, None),
            P(None, "tp"),
            P(None, "tp"),
            P("tp", None),
        ),
        out_specs=(P(("grp", "ep", "tp"), None), P(("grp", "ep", "tp"), None)),
        check_vma=False,
    )
```

profile of v0, /device:TPU:40, one launch (start us, length us, event | category | flops | bytes accessed | tf_op | source)
XLA Modules:
  0.0 298.8 jit_solution(3649183781875547081)
XLA Ops:
  0.6 0.0 copy-start
  0.6 0.8 broadcast_multiply_fusion
  1.5 0.8 copy.21
  2.2 0.1 eq.29
  2.4 0.1 eq.25
  2.5 1.1 fusion.20
  3.6 0.1 copy.20
  3.7 0.1 mul.154
  3.8 0.1 copy.23
  3.9 0.2 fusion.40
  4.2 0.2 fusion.42
  4.4 1.4 scatter_custom_fusion
  5.9 1.1 fusion.22
  6.9 3.1 %gather_fusion = bf16[384,2048]{1,0:T(8,128)(2,1)} fusion(bf16[64,2048]{1,0:T(8,128)(2,1)S(1)} %fusion.22, s32[1024]{0:T(1024)S(1)} %pad_clamp_fusion.1), kind=kCustom, calls=%fused_computation | custom fusion | bytes 3147264 | tf_op jit(solution)/shard_map/gather | solution.py:107
  10.0 5.1 %reshape.98 = bf16[128,3,2048]{2,1,0:T(4,128)(2,1)} reshape(bf16[384,2048]{1,0:T(8,128)(2,1)} %gather_fusion) | data formatting | bytes 3145728 | tf_op jit(solution)/shard_map/reshape | solution.py:107
  15.2 32.4 %all-to-all-start.1 = ((bf16[128,3,2048]{2,1,0:T(4,128)(2,1)}), bf16[128,3,2048]{2,1,0:T(4,128)(2,1)}, u32[]{:S(2)}, u32[]{:S(2)}) async-start(bf16[128,3,2048]{2,1,0:T(4,128)(2,1)} %reshape.98), calls=%async_computation.1 | async-start | bytes 4194304 | tf_op jit(solution)/shard_map/all_to_all | solution.py:108
  47.6 1.3 collective-permute-start
  48.9 2.1 collective-permute-start.1
  51.1 0.0 copy-start.8
  51.1 0.8 dynamic-slice_convert_fusion
  51.8 13.5 %all-gather.1 = bf16[128,2048]{1,0:T(8,128)(2,1)S(1)} all-gather(bf16[32,2048]{1,0:T(8,128)(2,1)S(1)} %get-tuple-element.5), channel_id=3, replica_groups=mesh['grp'=2,'ep'=32,'tp'=4] {'tp'}, dimensions={0}, use_global_device_ids=true | all-gather | bytes 655360 | tf_op jit(solution)/shard_map/all_gather | solution.py:28
  65.4 13.9 %all-gather = bf16[128,2048]{1,0:T(8,128)(2,1)S(1)} all-gather(bf16[32,2048]{1,0:T(8,128)(2,1)S(1)} %get-tuple-element.4), channel_id=2, replica_groups=mesh['grp'=2,'ep'=32,'tp'=4] {'tp'}, dimensions={0}, use_global_device_ids=true | all-gather | bytes 655360 | tf_op jit(solution)/shard_map/all_gather | solution.py:28
  79.3 0.3 fusion.31
  79.6 0.3 fusion.33
  79.9 0.3 fusion.12
  80.2 0.3 fusion.11
  80.5 0.4 convolution_convert_fusion.1
  81.0 0.1 convert_multiply_fusion.2
  81.1 0.7 copy-done.7
  81.8 0.8 convolution_convert_fusion.2
  82.6 1.5 pad_maximum_fusion
  84.1 59.2 %all-to-all-done.1 = bf16[128,3,2048]{2,1,0:T(4,128)(2,1)} async-done(((bf16[128,3,2048]{2,1,0:T(4,128)(2,1)}), bf16[128,3,2048]{2,1,0:T(4,128)(2,1)}, u32[]{:S(2)}, u32[]{:S(2)}) %all-to-all-start.1) | async-done | bytes 1572896 | tf_op jit(solution)/shard_map/all_to_all | solution.py:108
  143.3 4.7 %all-to-all-start = ((bf16[4,64,4096]{2,1,0:T(8,128)(2,1)}), bf16[4,64,4096]{2,1,0:T(8,128)(2,1)}, u32[]{:S(2)}, u32[]{:S(2)}) async-start(bf16[4,64,4096]{2,1,0:T(8,128)(2,1)} %pad_maximum_fusion), calls=%async_computation | async-start | bytes 4194304 | tf_op jit(solution)/shard_map/all_to_all | solution.py:40
  148.0 5.1 %reshape.99 = bf16[384,2048]{1,0:T(8,128)(2,1)} reshape(bf16[128,3,2048]{2,1,0:T(4,128)(2,1)} %all-to-all-done.1) | data formatting | bytes 3145728 | tf_op jit(solution)/shard_map/reshape | solution.py:109
  153.1 3.0 %fusion.3 = f32[384,512]{1,0:T(8,128)S(1)} fusion(bf16[384,2048]{1,0:T(8,128)(2,1)} %reshape.99, bf16[1,2048,512]{2,1,0:T(8,128)(2,1)} %param.26), kind=kOutput, calls=%fused_computation.11 | convolution fusion | flops 805306368 | bytes 4456448 | tf_op jit(solution)/shard_map/dot_general | solution.py:110
  156.1 5.2 %convolution_convert_fusion = bf16[384,2048]{1,0:T(8,128)(2,1)} fusion(bf16[1,512,2048]{2,1,0:T(8,128)(2,1)S(1)} %copy-done, bf16[384,2048]{1,0:T(8,128)(2,1)} %reshape.99, bf16[1,2048,512]{2,1,0:T(8,128)(2,1)} %param.27, f32[384,512]{1,0:T(8,128)S(1)} %fusion.3), kind=kOutput, calls=%fused_computation.4 | convolution fusion | flops 1612578816 | bytes 8126464 | tf_op jit(solution)/shard_map/dot_general | solution.py:113
  161.3 5.2 %reshape.100 = bf16[128,3,2048]{2,1,0:T(4,128)(2,1)} reshape(bf16[384,2048]{1,0:T(8,128)(2,1)} %convolution_convert_fusion) | data formatting | bytes 3145728 | tf_op jit(solution)/shard_map/reshape | solution.py:117
  166.5 8.2 %all-to-all-done = bf16[4,64,4096]{2,1,0:T(8,128)(2,1)} async-done(((bf16[4,64,4096]{2,1,0:T(8,128)(2,1)}), bf16[4,64,4096]{2,1,0:T(8,128)(2,1)}, u32[]{:S(2)}, u32[]{:S(2)}) %all-to-all-start) | async-done | bytes 2097184 | tf_op jit(solution)/shard_map/all_to_all | solution.py:40
  174.7 11.5 %all-to-all-start.2 = ((bf16[128,3,2048]{2,1,0:T(4,128)(2,1)}), bf16[128,3,2048]{2,1,0:T(4,128)(2,1)}, u32[]{:S(2)}, u32[]{:S(2)}) async-start(bf16[128,3,2048]{2,1,0:T(4,128)(2,1)} %reshape.100), calls=%async_computation.2 | async-start | bytes 4194304 | tf_op jit(solution)/shard_map/all_to_all | solution.py:116
  186.2 0.1 copy.19
  186.3 2.0 convert_reduce_fusion
  188.4 0.1 multiply_reduce_fusion.1
  188.5 93.4 %all-to-all-done.2 = bf16[128,3,2048]{2,1,0:T(4,128)(2,1)} async-done(((bf16[128,3,2048]{2,1,0:T(4,128)(2,1)}), bf16[128,3,2048]{2,1,0:T(4,128)(2,1)}, u32[]{:S(2)}, u32[]{:S(2)}) %all-to-all-start.2) | async-done | bytes 1572896 | tf_op jit(solution)/shard_map/all_to_all | solution.py:116
  281.9 5.0 %reshape.101 = bf16[384,2048]{1,0:T(8,128)(2,1)} reshape(bf16[128,3,2048]{2,1,0:T(4,128)(2,1)} %all-to-all-done.2) | data formatting | bytes 3145728 | tf_op jit(solution)/shard_map/reshape | solution.py:123
  287.0 5.0 %gather_fusion.1 = bf16[256,2048]{1,0:T(8,128)(2,1)} fusion(bf16[384,2048]{1,0:T(8,128)(2,1)} %reshape.101, s32[1024]{0:T(1024)S(1)} %pad_clamp_fusion), kind=kCustom, calls=%fused_computation.1 | custom fusion | bytes 2098176 | tf_op jit(solution)/shard_map/gather | solution.py:123
  291.9 2.7 reshape.102
  294.7 3.2 %multiply_reduce_fusion = f32[64,2048]{1,0:T(8,128)S(1)} fusion(f32[64,4,2048]{2,1,0:T(4,128)} %reshape.102, f32[64,4]{1,0:T(8,128)S(1)} %copy.19), kind=kLoop, calls=%fused_computation.13 | loop fusion | flops 917504 | bytes 2622464 | tf_op jit(solution)/shard_map/reduce_sum | solution.py:125
  297.9 0.9 fusion.23
  (36 shorter events, 0.2 us)
Async XLA Ops:
  0.6 155.5 %copy-start = (bf16[1,512,2048]{2,1,0:T(8,128)(2,1)S(1)}, bf16[1,512,2048]{2,1,0:T(8,128)(2,1)}, u32[]{:S(2)}) copy-start(bf16[1,512,2048]{2,1,0:T(8,128)(2,1)} %param.28) | copy-start | bytes 6291460
  15.2 32.4 %copy-start.3 = (bf16[256,512]{1,0:T(8,128)(2,1)S(1)}, bf16[256,512]{1,0:T(8,128)(2,1)}, u32[]{:S(2)}) copy-start(bf16[256,512]{1,0:T(8,128)(2,1)} %param.17) | copy-start | bytes 786436
  15.2 33.7 %copy-start.4 = (bf16[256,512]{1,0:T(8,128)(2,1)S(1)}, bf16[256,512]{1,0:T(8,128)(2,1)}, u32[]{:S(2)}) copy-start(bf16[256,512]{1,0:T(8,128)(2,1)} %param.18) | copy-start | bytes 786436
  15.2 64.1 %copy-start.1 = (bf16[2048,128]{1,0:T(8,128)(2,1)S(1)}, bf16[2048,128]{1,0:T(8,128)(2,1)}, u32[]{:S(2)}) copy-start(bf16[2048,128]{1,0:T(8,128)(2,1)} %param.29) | copy-start | bytes 1572868
  15.2 128.1 %all-to-all-start.1 = ((bf16[128,3,2048]{2,1,0:T(4,128)(2,1)}), bf16[128,3,2048]{2,1,0:T(4,128)(2,1)}, u32[]{:S(2)}, u32[]{:S(2)}) async-start(bf16[128,3,2048]{2,1,0:T(4,128)(2,1)} %reshape.98), calls=%async_computation.1 | async-start | bytes 4194304 | tf_op jit(solution)/shard_map/all_to_all | solution.py:108
  47.6 33.3 %collective-permute-start = (bf16[2,512]{1,0:T(2,128)(2,1)S(1)}, bf16[2,512]{1,0:T(2,128)(2,1)S(1)}, u32[]{:S(2)}, u32[]{:S(2)}) collective-permute-start(bf16[2,512]{1,0:T(2,128)(2,1)S(1)} %slice.43), channel_id=1, source_target_pairs={{0,4},{4,8},{8,12},{12,16},{16,20},{20,24},{24,28},{28,32},{32,36}... | collective-permute-start | bytes 6152 | tf_op jit(solution)/shard_map/ppermute | solution.py:12
  48.9 32.0 %collective-permute-start.1 = (bf16[2,512]{1,0:T(2,128)(2,1)S(1)}, bf16[2,512]{1,0:T(2,128)(2,1)S(1)}, u32[]{:S(2)}, u32[]{:S(2)}) collective-permute-start(bf16[2,512]{1,0:T(2,128)(2,1)S(1)} %slice.44), channel_id=1, source_target_pairs={{0,4},{4,8},{8,12},{12,16},{16,20},{20,24},{24,28},{28,32},{32,36}... | collective-permute-start | bytes 6152 | tf_op jit(solution)/shard_map/ppermute | solution.py:12
  51.1 28.8 %copy-start.8 = (bf16[2048,128]{1,0:T(8,128)(2,1)S(1)}, bf16[2048,128]{1,0:T(8,128)(2,1)}, u32[]{:S(2)}) copy-start(bf16[2048,128]{1,0:T(8,128)(2,1)} %param.30) | copy-start | bytes 1572868
  79.3 1.2 copy-start.2
  80.2 1.6 copy-start.7
  80.2 1.6 copy-start.9
  143.3 31.4 %all-to-all-start = ((bf16[4,64,4096]{2,1,0:T(8,128)(2,1)}), bf16[4,64,4096]{2,1,0:T(8,128)(2,1)}, u32[]{:S(2)}, u32[]{:S(2)}) async-start(bf16[4,64,4096]{2,1,0:T(8,128)(2,1)} %pad_maximum_fusion), calls=%async_computation | async-start | bytes 4194304 | tf_op jit(solution)/shard_map/all_to_all | solution.py:40
  166.5 19.8 %copy-start.6 = (f32[64,4]{0,1:T(4,128)S(1)}, f32[64,4]{0,1:T(4,128)}, u32[]{:S(2)}) copy-start(f32[64,4]{0,1:T(4,128)} %param.25) | copy-start | bytes 3076
  174.7 107.3 %all-to-all-start.2 = ((bf16[128,3,2048]{2,1,0:T(4,128)(2,1)}), bf16[128,3,2048]{2,1,0:T(4,128)(2,1)}, u32[]{:S(2)}, u32[]{:S(2)}) async-start(bf16[128,3,2048]{2,1,0:T(4,128)(2,1)} %reshape.100), calls=%async_computation.2 | async-start | bytes 4194304 | tf_op jit(solution)/shard_map/all_to_all | solution.py:116
  294.7 3.2 %copy-start.5 = (f32[2048]{0:T(1024)S(1)}, f32[2048]{0:T(1024)}, u32[]{:S(2)}) copy-start(f32[2048]{0:T(1024)} %param.21) | copy-start | bytes 24580
where the time goes:
time: 301 us; the launch traced here: 299 us
  waiting for transfers between devices  161 us (53%)
  starting transfers between devices  52 us (17%)
  local copies, waits for them, and re-layouts  34.8 us (12%)
  blocking collectives  27.4 us (9%)
  other arithmetic  12.2 us (4%)
  matrix products  10.6 us (4%)
    all_to_all x1, waiting for transfers between devices, on_device(): lax.all_to_all(result.reshape(expert_count, capacity, feature_width), ('e...  93.4 us
    all_to_all x1, waiting for transfers between devices, on_device(): lax.all_to_all(outgoing, ('ep', 'tp'), split_axis=0, concat_axis=0, tiled...  59.2 us
    all_to_all x1, starting transfers between devices, on_device(): lax.all_to_all(outgoing, ('ep', 'tp'), split_axis=0, concat_axis=0, tiled...  32.4 us
    all_gather x2, blocking collectives, work_in_pieces(): outs.append(jax.vmap(apply)(lax.all_gather(share, axis), starts))  27.4 us
    all_to_all x1, starting transfers between devices, on_device(): lax.all_to_all(result.reshape(expert_count, capacity, feature_width), ('e...  11.5 us
    all_to_all x1, waiting for transfers between devices, summed_on_arrival(): lax.all_to_all(pieces, axis, split_axis=0, concat_axis=0, tiled=True)  8.2 us
  transfers between devices with their start and end apart: 5, of which 3 were waited for; matrix products, arithmetic and copies ran while one was open for 9% of the time, Pallas kernels for 0%

commit v1 on v0

v1 whole, which is shorter than its diff:
```python
import functools

import jax
import jax.numpy as jnp
from jax import lax
from jax.experimental import pallas as pl
from jax.experimental.pallas import tpu as pltpu
from jax.sharding import PartitionSpec as P

EPSILON = 1e-06
CAP = 3
PAD = 8
BF = jnp.bfloat16
F32 = jnp.float32
MESH = pl.DeviceIdType.MESH


def scale_of(v):
    return lax.rsqrt(jnp.mean(v * v, axis=-1, keepdims=True) + EPSILON)


def kernel(
    steps,
    tp_count,
    tok_ref,
    egain_ref,
    route_ref,
    taps_ref,
    mgain_ref,
    og_ref,
    ig_ref,
    iv_ref,
    mixw_hbm,
    wg_hbm,
    wu_hbm,
    wd_hbm,
    sg_hbm,
    su_hbm,
    sd_hbm,
    mix_out,
    exp_out,
    mixw,
    wg,
    wu,
    wd,
    sg,
    su,
    sd,
    agbuf,
    rbuf,
    xsend,
    xin,
    act,
    ybuf,
    ret,
    sbuf,
    shi,
    slo,
    cbuf,
    cown,
    rsend,
    rrecv,
    halo,
    scaled,
    part,
    rs_a,
    rs_b,
    xs,
    w_sem,
    d_send,
    d_recv,
    t_send,
    t_recv,
    x_send,
    x_recv,
    y_send,
    y_recv,
    r_send,
    r_recv,
    h_send,
    h_recv,
    g_send,
    g_recv,
    q_send,
    q_recv,
):
    last = steps - 1
    nz = 2 * steps
    me = lax.axis_index("ep")
    t = lax.axis_index("tp")
    c = lax.rem(me, 2)
    z = me // 2
    ep_count = 2 * nz
    up = lax.rem(me + 2, ep_count)
    down = lax.rem(me + ep_count - 2, ep_count)
    up_dev = {"ep": up, "tp": t}
    down_dev = {"ep": down, "tp": t}
    right = {"ep": me, "tp": lax.rem(t + 1, tp_count)}
    left = {"ep": me, "tp": lax.rem(t + tp_count - 1, tp_count)}
    after = {"ep": lax.rem(me + 1, ep_count), "tp": t}
    cross = {"ep": lax.rem(me + ep_count + 2 * c - 1, ep_count), "tp": t}
    j_me = c * tp_count + t
    rows = tok_ref.shape[0]
    half = rows // 2
    width = tok_ref.shape[1]
    plane = 2 * tp_count
    slots = plane * PAD

    peers = []
    for dc in range(2):
        for dt in range(tp_count):
            if dc or dt:
                pc = lax.rem(c + dc, 2)
                pt = lax.rem(t + dt, tp_count)
                peers.append((pc * tp_count + pt, {"ep": 2 * z + pc, "tp": pt}))

    def rcopy(src, dst, ssem, rsem, dev):
        return pltpu.make_async_remote_copy(
            src_ref=src,
            dst_ref=dst,
            send_sem=ssem,
            recv_sem=rsem,
            device_id=dev,
            device_id_type=MESH,
        )

    loads = [
        pltpu.make_async_copy(s, d, w_sem.at[n])
        for n, (s, d) in enumerate(
            (
                (mixw_hbm, mixw),
                (sg_hbm, sg),
                (su_hbm, su),
                (sd_hbm, sd),
                (wg_hbm.at[0], wg),
                (wu_hbm.at[0], wu),
                (wd_hbm.at[0], wd),
            )
        )
    ]
    for load in loads:
        load.start()

    barrier = pltpu.get_barrier_semaphore()
    greeted = [up_dev, down_dev, cross] + [dev for _, dev in peers]
    for dev in greeted:
        pl.semaphore_signal(barrier, inc=1, device_id=dev, device_id_type=MESH)

    tok = tok_ref[...].astype(F32)
    agbuf[last, rows : 2 * rows, :] = (tok * scale_of(tok) * egain_ref[...]).astype(BF)
    rbuf[last, 1] = route_ref[...]
    pl.semaphore_wait(barrier, len(greeted))

    own = agbuf.at[last, pl.ds(rows, rows)]

    def ring_rows(way, h):
        return pl.ds(way * rows + h * half, half)

    ways = (up_dev, down_dev)

    def first_send(way, h):
        return rcopy(
            agbuf.at[last, pl.ds(rows + h * half, half)],
            agbuf.at[0, ring_rows(way, h)],
            d_send.at[way, h, 0],
            d_recv.at[way, h, 0],
            ways[way],
        )

    def ring_send(way, h, i):
        return rcopy(
            agbuf.at[i, ring_rows(way, h)],
            agbuf.at[i + 1, ring_rows(way, h)],
            d_send.at[way, h, i + 1],
            d_recv.at[way, h, i + 1],
            ways[way],
        )

    def last_send(way):
        return rcopy(
            agbuf.at[last - 1, ring_rows(way, way)],
            agbuf.at[last, pl.ds(way * half, half)],
            d_send.at[way, way, last],
            d_recv.at[way, way, last],
            ways[way],
        )

    def route_send(way, i):
        return rcopy(
            rbuf.at[i, way], rbuf.at[i + 1, way], t_send.at[way, i + 1], t_recv.at[way, i + 1], ways[way]
        )

    def route_first(way):
        return rcopy(
            rbuf.at[last, 1], rbuf.at[0, way], t_send.at[way, 0], t_recv.at[way, 0], ways[way]
        )

    for h in range(2):
        for way in range(2):
            first_send(way, h).start()
        if h == 0:
            for way in range(2):
                route_first(way).start()

    edge = ig_ref.shape[0] - 16
    halo_sends = [
        rcopy(src.at[pl.ds(edge, 16)], halo.at[n], h_send.at[n], h_recv.at[n], after)
        for n, src in enumerate((ig_ref, iv_ref))
    ]
    for s in halo_sends:
        s.start()
    gather = [
        rcopy(own, xs.at[3], g_send.at[0], g_recv.at[0], right),
        rcopy(own, xs.at[1], g_send.at[1], g_recv.at[1], left),
        rcopy(
            xs.at[3, pl.ds(0, half)], xs.at[2, pl.ds(0, half)], g_send.at[2], g_recv.at[2], right
        ),
        rcopy(
            xs.at[1, pl.ds(half, half)],
            xs.at[2, pl.ds(half, half)],
            g_send.at[3],
            g_recv.at[3],
            left,
        ),
    ]
    gather[0].start()
    gather[1].start()

    def block(k):
        return lax.rem(t + k, tp_count)

    def scatter_one(which):
        return [
            rcopy(
                part.at[which, block(2), pl.ds(0, half)],
                rs_a.at[which, 0],
                q_send.at[which, 0],
                q_recv.at[which, 0],
                right,
            ),
            rcopy(
                part.at[which, block(2), pl.ds(half, half)],
                rs_a.at[which, 1],
                q_send.at[which, 1],
                q_recv.at[which, 1],
                left,
            ),
            rcopy(
                part.at[which, block(1), pl.ds(half, half)],
                rs_b.at[which, 0, pl.ds(half, half)],
                q_send.at[which, 2],
                q_recv.at[which, 2],
                right,
            ),
            rcopy(
                part.at[which, block(3), pl.ds(0, half)],
                rs_b.at[which, 1, pl.ds(0, half)],
                q_send.at[which, 3],
                q_recv.at[which, 3],
                left,
            ),
        ]

    def scatter_two(which):
        return [
            rcopy(
                part.at[which, block(1), pl.ds(0, half)],
                rs_b.at[which, 0, pl.ds(0, half)],
                q_send.at[which, 4],
                q_recv.at[which, 4],
                right,
            ),
            rcopy(
                part.at[which, block(3), pl.ds(half, half)],
                rs_b.at[which, 1, pl.ds(half, half)],
                q_send.at[which, 5],
                q_recv.at[which, 5],
                left,
            ),
        ]

    def start_scatter(which):
        for s in scatter_one(which):
            s.start()

    def go_on_scatter(which):
        one, two = scatter_one(which), scatter_two(which)
        for n, (k, r) in enumerate(((1, 0), (3, half))):
            one[n].wait_recv()
            at = (which, block(k), pl.ds(r, half))
            part[at] = (part[at].astype(F32) + rs_a[which, n].astype(F32)).astype(BF)
            two[n].start()

    def end_scatter(which):
        one, two = scatter_one(which), scatter_two(which)
        for s in (one[2], one[3], two[0], two[1]):
            s.wait_recv()
        return (
            part[which, t].astype(F32)
            + rs_b[which, 0].astype(F32)
            + rs_b[which, 1].astype(F32)
        )

    def mixer():
        columns = ig_ref.shape[1]
        taps = taps_ref[:, pl.ds(pl.multiple_of(t * columns, columns), columns)].astype(F32)
        for s in halo_sends:
            s.wait_recv()
        ahead = halo[0].astype(F32) * halo[1].astype(F32)
        ahead = jnp.where(me > 0, ahead, 0.0)
        product = ig_ref[...].astype(F32) * iv_ref[...].astype(F32)
        number = lax.broadcasted_iota(jnp.int32, product.shape, 0)
        one = jnp.where(number == 0, ahead[15:16], pltpu.roll(product, 1, 0))
        two = pltpu.roll(product, 2, 0)
        two = jnp.where(number == 0, ahead[14:15], jnp.where(number == 1, ahead[15:16], two))
        filtered = taps[0:1] * two + taps[1:2] * one + taps[2:3] * product
        scaled[...] = (og_ref[...].astype(F32) * filtered).astype(BF)
        loads[0].wait()

        @pl.loop(0, tp_count)
        def _(b):
            lhs = scaled[pl.ds(pl.multiple_of(b * rows, rows), rows), :]
            for n in range(width // 512):
                at = pl.ds(n * 512, 512)
                part[0, b, :, at] = jnp.dot(
                    lhs, mixw[:, at], preferred_element_type=F32
                ).astype(BF)

    def shared():
        gather[2].wait_recv()
        gather[3].wait_recv()
        for n in (1, 2, 3):
            loads[n].wait()

        @pl.loop(0, tp_count)
        def _(k):
            b = block(k)
            lhs = xs[k]
            gate = jnp.dot(lhs, sg[...], preferred_element_type=F32)
            upper = jnp.dot(lhs, su[...], preferred_element_type=F32)
            hidden = (jax.nn.silu(gate) * upper).astype(BF)
            for n in range(width // 512):
                at = pl.ds(n * 512, 512)
                part[1, b, :, at] = jnp.dot(
                    hidden, sd[:, at], preferred_element_type=F32
                ).astype(BF)

    def select(i):
        lane = lax.broadcasted_iota(jnp.int32, (PAD, 2 * rows), 1)
        route = jnp.where(lane < rows, rbuf[i, 0], rbuf[i, 1])
        row = lax.broadcasted_iota(jnp.int32, (slots, 2 * rows), 0)
        col = lax.broadcasted_iota(jnp.int32, (slots, 2 * rows), 1)
        place = lax.rem(row, PAD)
        expert = (z * plane + row // PAD).astype(F32)
        hit = jnp.zeros((slots, 2 * rows), F32)
        weight = jnp.zeros((slots, 2 * rows), F32)
        for k in range(4):
            same = expert == route[k : k + 1]
            hit = jnp.where(same, 1.0, hit)
            weight = jnp.where(same, route[4 + k : 5 + k], weight)
        side = (place // CAP) == (col // rows)
        hit = jnp.where(side, hit, 0.0)
        order = lax.broadcasted_iota(jnp.int32, (2 * rows, 2 * rows), 0)
        later = lax.broadcasted_iota(jnp.int32, (2 * rows, 2 * rows), 1)
        below = jnp.where(order < later, 1.0, 0.0).astype(BF)
        rank = jnp.dot(hit.astype(BF), below, preferred_element_type=F32)
        hit = jnp.where(rank == lax.rem(place, CAP).astype(F32), hit, 0.0)
        weight = weight * hit
        high = weight.astype(BF)
        shi[i] = high
        slo[i] = (weight - high.astype(F32)).astype(BF)
        sbuf[...] = hit.astype(BF)
        for n in range(width // 512):
            at = pl.ds(n * 512, 512)
            got = jnp.dot(sbuf[...], agbuf[i, :, at], preferred_element_type=F32)
            xsend[i, :, :, at] = got.reshape(plane, PAD, 512).astype(BF)
        xin[i, j_me] = xsend[i, j_me]
        for j, dev in peers:
            rcopy(xsend.at[i, j], xin.at[i, j_me], x_send.at[i], x_recv.at[i], dev).start()

    def all_peers(buf, i, sem):
        ref = buf.at[i, pl.ds(0, plane - 1)]
        return pltpu.make_async_copy(ref, ref, sem.at[i])

    def expert(i):
        all_peers(xin, i, x_recv).wait()
        lhs = xin[i].reshape(slots, width)
        for n in range(act.shape[1] // 256):
            at = pl.ds(n * 256, 256)
            gate = jnp.dot(lhs, wg[:, at], preferred_element_type=F32)
            upper = jnp.dot(lhs, wu[:, at], preferred_element_type=F32)
            act[:, at] = (jax.nn.silu(gate) * upper).astype(BF)
        for n in range(width // 512):
            at = pl.ds(n * 512, 512)
            got = jnp.dot(act[...], wd[:, at], preferred_element_type=F32)
            ybuf[i, :, :, at] = got.reshape(plane, PAD, 512).astype(BF)

    def give_back(i):
        ret[i, j_me] = ybuf[i, j_me]
        for j, dev in peers:
            rcopy(ybuf.at[i, j], ret.at[i, j_me], y_send.at[i], y_recv.at[i], dev).start()

    mixer()
    start_scatter(0)
    for n in (4, 5, 6):
        loads[n].wait()

    @pl.loop(0, steps)
    def _(i):
        for h in range(2):
            for way in range(2):

                @pl.when(i < last)
                def _():
                    rcopy(
                        agbuf.at[i, ring_rows(way, h)],
                        agbuf.at[i, ring_rows(way, h)],
                        d_send.at[way, h, i],
                        d_recv.at[way, h, i],
                        ways[way],
                    ).wait_recv()

                @pl.when(i < last - 1)
                def _():
                    ring_send(way, h, i).start()

                if h == way:

                    @pl.when(i == last - 1)
                    def _():
                        last_send(way).start()

                    @pl.when(i == last)
                    def _():
                        last_send(way).wait_recv()

            if h == 0:
                for way in range(2):

                    @pl.when(i < last)
                    def _():
                        rcopy(
                            rbuf.at[i, way],
                            rbuf.at[i, way],
                            t_send.at[way, i],
                            t_recv.at[way, i],
                            ways[way],
                        ).wait_recv()

                    @pl.when(i < last - 1)
                    def _():
                        route_send(way, i).start()

                @pl.when(i == last - 1)
                def _():
                    route_send(0, i).start()

                @pl.when(i == last)
                def _():
                    rcopy(
                        rbuf.at[i, 0], rbuf.at[i, 0], t_send.at[0, i], t_recv.at[0, i], ways[0]
                    ).wait_recv()

                @pl.when(i == 0)
                def _():
                    xs[0] = own[...]
                    gather[0].wait_recv()
                    gather[2].start()
                    gather[1].wait_recv()
                    gather[3].start()

                @pl.when(i == 1)
                def _():
                    shared()

                @pl.when(i >= 2)
                def _():
                    expert(i - 2)

                @pl.when(i == 2)
                def _():
                    go_on_scatter(0)

        select(i)

    expert(last - 1)
    expert(last)
    give_back(last)
    give_back(last - 1)
    give_back(last - 2)

    def combine(i, slot):
        all_peers(ret, i, y_recv).wait()
        for n in range(width // 512):
            at = pl.ds(n * 512, 512)
            rhs = ret[i, :, :, at].reshape(slots, 512)
            turn = (((0,), (0,)), ((), ()))
            got = lax.dot_general(shi[i], rhs, turn, preferred_element_type=F32)
            got += lax.dot_general(slo[i], rhs, turn, preferred_element_type=F32)
            cbuf[slot, :, at] = got

    back = (down_dev, up_dev)

    def back_send(way, h, i):
        return rcopy(
            rsend.at[i, ring_rows(way, h)],
            rrecv.at[i, ring_rows(way, h)],
            r_send.at[way, h, i],
            r_recv.at[way, h, i],
            back[way],
        )

    def back_last(way):
        return rcopy(
            rsend.at[last, pl.ds(way * half, half)],
            rrecv.at[last, ring_rows(way, way)],
            r_send.at[way, way, last],
            r_recv.at[way, way, last],
            back[way],
        )

    combine(last, 0)
    for way in range(2):
        at = pl.ds(way * half, half)
        rsend[last, at] = cbuf[0, at].astype(BF)
        back_last(way).start()
    cown[...] = cbuf[0, rows : 2 * rows]
    combine(last - 1, 1)

    @pl.loop(0, last)
    def _(n):
        i = last - 1 - n
        slot = lax.rem(n + 1, 2)

        @pl.when(i >= 2)
        def _():
            give_back(i - 2)

        for h in range(2):
            for way in range(2):
                at = ring_rows(way, h)
                if h == way:

                    @pl.when(i == last - 1)
                    def _():
                        back_last(way).wait_recv()

                @pl.when(i < last - 1)
                def _():
                    back_send(way, h, i + 1).wait_recv()

                if h == way:
                    total = cbuf[slot, at] + rrecv[i + 1, at].astype(F32)
                    rsend[i, at] = total.astype(BF)
                else:

                    @pl.when(i < last - 1)
                    def _():
                        total = cbuf[slot, at] + rrecv[i + 1, at].astype(F32)
                        rsend[i, at] = total.astype(BF)

                    @pl.when(i == last - 1)
                    def _():
                        rsend[i, at] = cbuf[slot, at].astype(BF)

                back_send(way, h, i).start()
            if h == 0:

                @pl.when(i > 0)
                def _():
                    combine(i - 1, 1 - slot)

        @pl.when(n == 1)
        def _():
            start_scatter(1)

        @pl.when(n == 3)
        def _():
            go_on_scatter(1)

    mixed = end_scatter(0)
    mix_out[...] = (mixed * scale_of(mixed) * mgain_ref[...]).astype(BF)
    cown[...] = cown[...] + end_scatter(1)
    for h in range(2):
        for way in range(2):
            back_send(way, h, 0).wait_recv()
    exp_out[...] = (
        cown[...] + rrecv[0, 0:rows].astype(F32) + rrecv[0, rows : 2 * rows].astype(F32)
    ).astype(BF)

    for s in halo_sends + gather:
        s.wait_send()
    for which in range(2):
        for s in scatter_one(which) + scatter_two(which):
            s.wait_send()
    for way in range(2):
        last_send(way).wait_send()
        back_last(way).wait_send()
    route_send(0, last - 1).wait_send()

    @pl.loop(0, steps)
    def _(i):
        all_peers(xin, i, x_send).wait()
        all_peers(xin, i, y_send).wait()

        @pl.when(i < last)
        def _():
            for way in range(2):
                rcopy(
                    rbuf.at[i, way], rbuf.at[i, way], t_send.at[way, i], t_recv.at[way, i], ways[way]
                ).wait_send()
                for h in range(2):
                    rcopy(
                        agbuf.at[i, ring_rows(way, h)],
                        agbuf.at[i, ring_rows(way, h)],
                        d_send.at[way, h, i],
                        d_recv.at[way, h, i],
                        ways[way],
                    ).wait_send()
                    back_send(way, h, i).wait_send()


def on_device(
    outer_gate,
    inner_gate,
    inner_value,
    conv_taps,
    mixer_out,
    mixer_gain,
    moe_tokens,
    expert_gain,
    route_ids,
    route_weights,
    expert_gate,
    expert_up,
    expert_down,
    shared_gate,
    shared_up,
    shared_down,
):
    ep_count = lax.axis_size("ep")
    tp_count = lax.axis_size("tp")
    steps = ep_count // 4
    plane = 2 * tp_count
    rows, width = moe_tokens.shape
    half = rows // 2
    hidden = expert_gate.shape[2]
    route = jnp.concatenate([route_ids.astype(F32).T, route_weights.T], axis=0)
    route = jnp.concatenate([route, route], axis=1)
    vm = pl.BlockSpec(memory_space=pltpu.VMEM)
    hbm = pl.BlockSpec(memory_space=pl.ANY)
    dma = pltpu.SemaphoreType.DMA
    scratch = [
        pltpu.VMEM(mixer_out.shape, BF),
        pltpu.VMEM(expert_gate.shape[1:], BF),
        pltpu.VMEM(expert_up.shape[1:], BF),
        pltpu.VMEM(expert_down.shape[1:], BF),
        pltpu.VMEM(shared_gate.shape, BF),
        pltpu.VMEM(shared_up.shape, BF),
        pltpu.VMEM(shared_down.shape, BF),
        pltpu.VMEM((steps, 2 * rows, width), BF),
        pltpu.VMEM((steps, 2, PAD, 2 * rows), F32),
        pltpu.VMEM((steps, plane, PAD, width), BF),
        pltpu.VMEM((steps, plane, PAD, width), BF),
        pltpu.VMEM((plane * PAD, hidden), BF),
        pltpu.VMEM((steps, plane, PAD, width), BF),
        pltpu.VMEM((steps, plane, PAD, width), BF),
        pltpu.VMEM((plane * PAD, 2 * rows), BF),
        pltpu.VMEM((steps, plane * PAD, 2 * rows), BF),
        pltpu.VMEM((steps, plane * PAD, 2 * rows), BF),
        pltpu.VMEM((2, 2 * rows, width), F32),
        pltpu.VMEM((rows, width), F32),
        pltpu.VMEM((steps, 2 * rows, width), BF),
        pltpu.VMEM((steps, 2 * rows, width), BF),
        pltpu.VMEM((2, 16, inner_gate.shape[1]), BF),
        pltpu.VMEM(inner_gate.shape, BF),
        pltpu.VMEM((2, tp_count, rows, width), BF),
        pltpu.VMEM((2, 2, half, width), BF),
        pltpu.VMEM((2, 2, rows, width), BF),
        pltpu.VMEM((tp_count, rows, width), BF),
        dma((7,)),
        dma((2, 2, steps)),
        dma((2, 2, steps)),
        dma((2, steps)),
        dma((2, steps)),
        dma((steps,)),
        dma((steps,)),
        dma((steps,)),
        dma((steps,)),
        dma((2, 2, steps)),
        dma((2, 2, steps)),
        dma((2,)),
        dma((2,)),
        dma((4,)),
        dma((4,)),
        dma((2, 6)),
        dma((2, 6)),
    ]
    out = jax.ShapeDtypeStruct((rows, width), BF)
    return pl.pallas_call(
        functools.partial(kernel, steps, tp_count),
        out_shape=(out, out),
        in_specs=[vm] * 8 + [hbm] * 7,
        out_specs=(vm, vm),
        scratch_shapes=scratch,
        compiler_params=pltpu.CompilerParams(
            collective_id=0, has_side_effects=True, vmem_limit_bytes=60 * 1024 * 1024
        ),
        name="layer",
    )(
        moe_tokens,
        expert_gain.reshape(1, -1),
        route,
        conv_taps,
        mixer_gain.reshape(1, -1),
        outer_gate,
        inner_gate,
        inner_value,
        mixer_out,
        expert_gate,
        expert_up,
        expert_down,
        shared_gate,
        shared_up,
        shared_down,
    )


def solution(mesh):
    return jax.shard_map(
        on_device,
        mesh=mesh,
        in_specs=(
            P(("grp", "ep"), "tp"),
            P(("grp", "ep"), "tp"),
            P(("grp", "ep"), "tp"),
            P(),
            P("tp", None),
            P(),
            P(("grp", "ep", "tp"), None),
            P(),
            P(("grp", "ep", "tp"), None),
            P(("grp", "ep", "tp"), None),
            P(("ep", "tp"), None, None),
            P(("ep", "tp"), None, None),
            P(("ep", "tp"), None, None),
            P(None, "tp"),
            P(None, "tp"),
            P("tp", None),
        ),
        out_specs=(P(("grp", "ep", "tp"), None), P(("grp", "ep", "tp"), None)),
        check_vma=False,
    )
```

time: 301 us -> 149 us (0.50)
  waiting for transfers between devices: 161 us -> 0 us
  Pallas kernels: 0 us -> 141 us
  starting transfers between devices: 52 us -> 0 us
  local copies, waits for them, and re-layouts: 34.8 us -> 3.34 us
  blocking collectives: 27.4 us -> 0 us
  matrix products: 10.6 us -> 0 us
  other arithmetic: 12.2 us -> 2.11 us
    all_to_all x3 -> x0, waiting for transfers between devices: 161 us -> none  [the longest x1 93.4 us: on_device(): lax.all_to_all(result.reshape(expert_count, capacity, feature_width), ('e...]
    pallas_call x0 -> x1, Pallas kernels: none -> 141 us  [on_device(): pl.pallas_call(functools.partial(kernel, steps, tp_count), out_shape=(out...]
    all_to_all x3 -> x0, starting transfers between devices: 48.6 us -> none  [the longest x1 32.4 us: on_device(): lax.all_to_all(outgoing, ('ep', 'tp'), split_axis=0, concat_axis=0, tiled...]
    all_gather x2 -> x0, blocking collectives: 27.4 us -> none  [work_in_pieces(): outs.append(jax.vmap(apply)(lax.all_gather(share, axis), starts))]
    reshape x4 -> x0, local copies, waits for them, and re-layouts: 20.4 us -> none  [the longest x1 5.16 us: on_device(): result.reshape(expert_count, capacity, feature_width)]
    dot_general x8 -> x0, matrix products: 10.6 us -> none  [the longest x1 5.2 us: on_device(): jnp.dot(active, expert_down[0], preferred_element_type=jnp.float32)]
    gather x2 -> x0, local copies, waits for them, and re-layouts: 8.06 us -> none  [the longest x1 4.96 us: on_device(): returned.reshape(expert_count * capacity, feature_width)[target]]
    reduce_sum x5 -> x0, other arithmetic: 6.63 us -> none  [the longest x1 3.18 us: on_device(): jnp.sum((weights[:, None] * picked).reshape(row_count, top_count, feature...]
  transfers between devices with their start and end apart: 5 -> 0, of which waited for: 3 -> 0; matrix products, arithmetic and copies ran while one was open for 9% -> 0% of each run, Pallas kernels for 0% -> 0%
where the time goes in v1:
time: 149 us; the launch traced here: 147 us
  Pallas kernels  141 us (95%)
  local copies, waits for them, and re-layouts  3.34 us (2%)
  other arithmetic  2.11 us (1%)
    pallas_call x1, Pallas kernels, on_device(): pl.pallas_call(functools.partial(kernel, steps, tp_count), out_shape=(out...  141 us
    unnamed x2, local copies, waits for them, and re-layouts  3.34 us

profile of v1, /device:TPU:40, one launch (start us, length us, event | category | flops | bytes accessed | tf_op | source)
XLA Modules:
  0.0 147.4 jit_solution(16262128412653690300)
XLA Ops:
  0.6 0.7 convert_bitcast_fusion
  1.3 1.4 maximum_maximum_fusion.route_ref
  2.7 141.4 %layer.1 = (bf16[64,2048]{1,0:T(8,128)(2,1)}, bf16[64,2048]{1,0:T(8,128)(2,1)}) custom-call(bf16[64,2048]{1,0:T(8,128)(2,1)} %tok_ref.1, f32[1,2048]{1,0:T(1,128)} %bitcast.5, f32[8,128]{1,0:T(8,128)} %maximum_maximum_fusion.route_ref, bf16[3,2048]{1,0:T(4,128)(2,1)} %taps_ref.1, f32[1,2048]{1,0:T(1,128)} %bitcast.6, bf16[256,512]{1,0:T(8,128)(2,1)} %og_ref.1, ...), custom_call_target="tpu_custom_call" | custom-call | tf_op jit(solution)/shard_map/layer/pallas_call | solution.py:700
  144.1 1.7 %copy.20 = bf16[64,2048]{1,0:T(8,128)(2,1)} copy(bf16[64,2048]{1,0:T(8,128)(2,1)} %get-tuple-element.4) | data formatting | bytes 524288
  145.8 1.7 %copy.21 = bf16[64,2048]{1,0:T(8,128)(2,1)} copy(bf16[64,2048]{1,0:T(8,128)(2,1)} %get-tuple-element.5) | data formatting | bytes 524288
